TPU v7x, 256 devices: a 4x2x16 block of a 4x16x16 slice. The times are simulated.
256 devices in a mesh: grp: 2 (over y), kv: 32 (over z, core), tp: 4 (over x).
Axes of the slice: x: 4, y: 2, z: 16, core: 2. Of those that a mesh axis runs over, the one named last changes fastest.
The devices are a block of a 4x16x16 slice.
Arguments:
- hidden: bfloat16 [2048, 4096], P('grp', 'kv'), parts along dimension 0, may hold values from -64 to 64
- norm_gain: bfloat16 [4096], replicated, may hold values from 0.099609375 to 1.8984375
- w_query: bfloat16 [4096, 2048], P('kv', 'tp'), may hold values from -0.09375 to 0.09375
- w_key: bfloat16 [4096, 2048], P('kv', 'tp'), may hold values from -0.09375 to 0.09375
- w_value: bfloat16 [4096, 2048], P('kv', 'tp'), may hold values from -0.09375 to 0.09375
- w_gate: bfloat16 [4096, 2048], P('kv', 'tp'), may hold values from -0.09375 to 0.09375
- w_decay: bfloat16 [4096, 16], P(None, 'tp'), may hold values from -0.09375 to 0.09375
- w_write: bfloat16 [4096, 16], P(None, 'tp'), may hold values from -0.09375 to 0.09375
- decay_rate: float32 [16], P('tp'), may hold values from 0.02 to 1
- head_gain: bfloat16 [128], replicated, may hold values from 0.099609375 to 1.8984375
- w_output: bfloat16 [2048, 4096], P('tp', 'kv'), may hold values from -0.125 to 0.125
- state: float32 [512, 16, 16384], P(('grp', 'kv'), 'tp'), parts along dimension 0, may hold values from -6 to 6
- prev_keys: bfloat16 [512, 4, 2048], P(('grp', 'kv'), None, 'tp'), parts along dimension 0, may hold values from -6 to 6
- prev_values: bfloat16 [512, 4, 2048], P(('grp', 'kv'), None, 'tp'), parts along dimension 0, may hold values from -6 to 6
- prev_decay: float32 [512, 4, 16], P(('grp', 'kv'), None, 'tp'), parts along dimension 0, may hold values from -1 to -0.02
- prev_write: float32 [512, 4, 16], P(('grp', 'kv'), None, 'tp'), parts along dimension 0, may hold values from 0.05 to 0.95
- accepted: int32 [512], P(('grp', 'kv')), parts along dimension 0, may hold values from 0 to 4
Outputs:
- mixed: bfloat16 [2048, 4096], P('grp', 'kv'), parts along dimension 0
- state_out: float32 [512, 16, 16384], P(('grp', 'kv'), 'tp'), parts along dimension 0
There are 2 independent parts, one for each index of `grp`. A program takes and returns all parts, laid end to end along the dimension named above; an argument that names none is the same for every part. Nothing has to cross between parts.
All inputs are finite; a program needn't handle non-finite values.
Results may differ from a plain program's by a relative error of at most 0.0069.
Values may be sent and summed in bfloat16 or wider, within the bound.
A program may use at most 64 MiB of HBM per device.

v0:
```python
import jax
import jax.numpy as jnp
from jax import lax
from jax.sharding import Mesh
from jax.sharding import PartitionSpec as P

KV = ("kv_0", "kv_1")
GRP_KV = ("grp", "kv_0", "kv_1")
EPSILON = 1e-06


def side_by_side(arrays, axis, dim, along):
    ends, at = ([], 0)
    for a in arrays[:-1]:
        at += a.shape[along]
        ends.append(at)
    both = jnp.concatenate(arrays, axis=along)
    return tuple(jnp.split(lax.all_gather(both, axis, axis=dim, tiled=True), ends, axis=along))


def in_order(tiles, dim):
    tiles = jnp.moveaxis(tiles, 0, dim)
    shape = tiles.shape
    return tiles.reshape(*shape[:dim], shape[dim] * shape[dim + 1], *shape[dim + 2 :])


def gather_in_order(value, axes, turns):
    tiles = value[None]
    for k in turns:
        tiles = lax.all_gather(tiles, axes[k], axis=0, tiled=True)
    block = [lax.axis_size(axes[k]) for k in reversed(turns)]
    tiles = tiles.reshape(*block, *value.shape)
    turned = sorted(range(len(turns)), key=lambda place: turns[len(turns) - 1 - place])
    return tiles.transpose(*turned, *range(len(turns), tiles.ndim)).reshape(-1, *value.shape)


def whole_of(value, axes, turns, dim):
    return in_order(gather_in_order(value, axes, turns), dim)


def from_everyone(value, axis):
    copies = jnp.broadcast_to(value, (lax.axis_size(axis), *value.shape))
    return lax.all_to_all(copies, axis, split_axis=0, concat_axis=0, tiled=True)


def of_everyone(value, axis):
    return from_everyone(value, axis).sum(axis=0)


def unit_rows(values):
    return values * lax.rsqrt(jnp.sum(values * values, axis=-1, keepdims=True) + EPSILON)


def delta_block(carried_state, keys, values, log_decay, writes, query_rows):
    length = keys.shape[2]
    totals = jnp.cumsum(log_decay, axis=-1)
    spread = totals[..., :, None] - totals[..., None, :]
    lower = jnp.tril(jnp.ones((length, length), dtype=bool))
    strict = jnp.tril(jnp.ones((length, length), dtype=bool), -1)
    within = jnp.where(lower, jnp.exp(jnp.where(lower, spread, 0.0)), 0.0)
    affinity = jnp.einsum("shid,shjd->shij", keys, keys, precision=lax.Precision.HIGHEST)
    coupling = jnp.where(strict, writes[..., :, None] * affinity * within, 0.0)
    source = jnp.concatenate(
        [values * writes[..., None], keys * (writes * jnp.exp(totals))[..., None]], axis=-1
    )
    solved = []
    for token_position in range(length):
        current = source[:, :, token_position]
        for earlier in range(token_position):
            current = current - coupling[:, :, token_position, earlier][..., None] * solved[earlier]
        solved.append(current)
    solved = jnp.stack(solved, axis=2)
    head_size = keys.shape[-1]
    fresh = solved[..., :head_size] - jnp.einsum(
        "shpk,shkv->shpv", solved[..., head_size:], carried_state, precision=lax.Precision.HIGHEST
    )
    outputs = None
    if query_rows is not None:
        scores = (
            jnp.einsum("shid,shjd->shij", query_rows, keys, precision=lax.Precision.HIGHEST)
            * within
        )
        outputs = jnp.einsum(
            "shpk,shkv->shpv",
            query_rows * jnp.exp(totals)[..., None],
            carried_state,
            precision=lax.Precision.HIGHEST,
        )
        outputs = outputs + jnp.einsum(
            "shij,shjv->shiv", scores, fresh, precision=lax.Precision.HIGHEST
        )
    final = totals[..., -1:]
    carried_state = carried_state * jnp.exp(final)[..., None] + jnp.einsum(
        "shpk,shpv->shkv",
        keys * jnp.exp(final - totals)[..., None],
        fresh,
        precision=lax.Precision.HIGHEST,
    )
    return (carried_state, outputs)


def per_device(
    hidden,
    norm_gain,
    w_query,
    w_key,
    w_value,
    w_gate,
    w_decay,
    w_write,
    decay_rate,
    head_gain,
    w_output,
    state,
    prev_keys,
    prev_values,
    prev_decay,
    prev_write,
    accepted,
):
    heads = w_decay.shape[1]
    width = w_query.shape[1]
    head_size = width // heads
    token_block = lax.all_to_all(hidden, KV, split_axis=0, concat_axis=1, tiled=True)
    wide = token_block.astype(jnp.float32)
    scaled = (wide * norm_gain.astype(jnp.float32)).astype(jnp.bfloat16)
    squares = jnp.sum(wide * wide, axis=1)
    pieces = side_by_side((w_query, w_key, w_value, w_gate), KV, 0, 1)
    summed = tuple((jnp.dot(scaled, piece, preferred_element_type=jnp.float32) for piece in pieces))
    projected = jnp.concatenate(summed, axis=1)
    small = jnp.dot(
        scaled, jnp.concatenate([w_decay, w_write], axis=1), preferred_element_type=jnp.float32
    )
    inverse = lax.rsqrt(squares / norm_gain.shape[0] + EPSILON)
    projected = projected * inverse[:, None]
    small = small * inverse[:, None]
    seqs = state.shape[0]
    proposals = projected.shape[0] // seqs

    def heads_first(block):
        return block.reshape(seqs, proposals, heads, head_size).transpose(0, 2, 1, 3)

    query_rows = unit_rows(heads_first(projected[:, :width])) * head_size ** (-0.5)
    keys = unit_rows(heads_first(projected[:, width : 2 * width]))
    values = heads_first(projected[:, 2 * width : 3 * width])
    gates = projected[:, 3 * width :].reshape(seqs, proposals, heads, head_size)
    log_decay = (
        (-decay_rate * jax.nn.softplus(small[:, :heads]))
        .reshape(seqs, proposals, heads)
        .transpose(0, 2, 1)
    )
    writes = jax.nn.sigmoid(small[:, heads:]).reshape(seqs, proposals, heads).transpose(0, 2, 1)
    taken = jnp.arange(proposals, dtype=jnp.int32)[None, :] < accepted[:, None]
    old_keys = unit_rows(
        prev_keys.astype(jnp.float32)
        .reshape(seqs, proposals, heads, head_size)
        .transpose(0, 2, 1, 3)
    )
    old_values = (
        prev_values.astype(jnp.float32)
        .reshape(seqs, proposals, heads, head_size)
        .transpose(0, 2, 1, 3)
    )
    old_decay = jnp.where(taken[:, :, None], prev_decay, 0.0).transpose(0, 2, 1)
    old_writes = jnp.where(taken[:, :, None], prev_write, 0.0).transpose(0, 2, 1)
    carried_state = state.reshape(seqs, heads, head_size, head_size)
    carried_state, _ = delta_block(carried_state, old_keys, old_values, old_decay, old_writes, None)
    _, outputs = delta_block(carried_state, keys, values, log_decay, writes, query_rows)
    outputs = outputs.transpose(0, 2, 1, 3)
    normed = outputs * lax.rsqrt(jnp.mean(outputs * outputs, axis=-1, keepdims=True) + EPSILON)
    normed = normed * head_gain.astype(jnp.float32) * jax.nn.silu(gates)
    heads_out = normed.reshape(seqs * proposals, width).astype(jnp.bfloat16)
    terms = jnp.dot(
        whole_of(heads_out, KV, (0, 1), 0), w_output, preferred_element_type=jnp.float32
    )
    mixed = of_everyone(terms, "tp").astype(jnp.bfloat16)
    return (mixed, carried_state.reshape(seqs, heads, head_size * head_size))


def solution(mesh):
    torus = Mesh(
        mesh.devices.reshape(mesh.shape["grp"], 16, 2, mesh.shape["tp"]),
        ("grp", "kv_0", "kv_1", "tp"),
    )
    in_specs = (
        P("grp", KV),
        P(),
        P(KV, "tp"),
        P(KV, "tp"),
        P(KV, "tp"),
        P(KV, "tp"),
        P(None, "tp"),
        P(None, "tp"),
        P("tp"),
        P(),
        P("tp", KV),
        P(GRP_KV, "tp", None),
        P(GRP_KV, None, "tp"),
        P(GRP_KV, None, "tp"),
        P(GRP_KV, None, "tp"),
        P(GRP_KV, None, "tp"),
        P(GRP_KV),
    )
    out_specs = (P("grp", KV), P(GRP_KV, "tp", None))
    return jax.shard_map(
        per_device, mesh=torus, in_specs=in_specs, out_specs=out_specs, check_vma=False
    )
```

profile of v0, /device:TPU:33, one launch (start us, length us, event | category | flops | bytes accessed | tf_op | source)
XLA Modules:
  0.0 251.3 jit_solution(17397073867392320041)
XLA Ops:
  7.3 2.0 pad_maximum_fusion
  9.4 25.5 %all-to-all-start = ((bf16[32,32,128]{2,1,0:T(8,128)(2,1)}), bf16[32,32,128]{2,1,0:T(8,128)(2,1)S(1)}, u32[]{:S(2)}, u32[]{:S(2)}) async-start(bf16[32,32,128]{2,1,0:T(8,128)(2,1)} %bitcast.155), calls=%async_computation | async-start | bytes 524288 | tf_op jit(solution)/shard_map/all_to_all | solution.py:124
  35.6 0.4 fusion.11
  36.2 0.2 fusion.79
  36.5 2.7 %reshape.141 = f32[8,4,128,128]{3,2,1,0:T(8,128)S(1)} reshape(f32[8,4,16384]{2,1,0:T(4,128)} %param.28) | data formatting | bytes 4194304 | tf_op jit(solution)/shard_map/reshape | solution.py:166
  40.5 0.3 multiply_subtract_fusion.2
  40.9 1.9 convolution_subtract_fusion.1
  42.8 5.3 %multiply_add_fusion = f32[8,4,128,128]{3,2,1,0:T(8,128)S(1)} fusion(f32[8,4,128,128]{3,2,1,0:T(8,128)} %copy-done.1, f32[8,4,4,128]{3,2,1,0:T(4,128)S(1)} %convolution_subtract_fusion.1, f32[8,4]{1,0:T(8,128)S(1)} %copy.352, bf16[8,4,512]{2,1,0:T(4,128)(2,1)S(1)} %copy-done.2, f32[8,4,4]{2,1,0:T(4,128)S(1)} %copy.353, f32[8,4,4]{2,1,0:T(4,128)S(1)} %add_rsqrt_fusion.2), kind=kOutput, calls=%fused_computation.8 | convolution fusion | flops 26263552 | bytes 4293760 | tf_op jit(solution)/shard_map/shpk,shpv->shkv/dot_general | solution.py:93
  48.1 10.1 %all-to-all-done = bf16[32,32,128]{2,1,0:T(8,128)(2,1)S(1)} async-done(((bf16[32,32,128]{2,1,0:T(8,128)(2,1)}), bf16[32,32,128]{2,1,0:T(8,128)(2,1)S(1)}, u32[]{:S(2)}, u32[]{:S(2)}) %all-to-all-start) | async-done | bytes 262176 | tf_op jit(solution)/shard_map/all_to_all | solution.py:124
  58.2 0.2 fusion.12
  58.4 0.2 convolution_multiply_fusion.3
  58.7 0.7 reduce_window_sum.17
  59.5 76.6 %all-gather.3.cloned.1.call-done = bf16[4096,2048]{1,0:T(8,128)(2,1)} async-done(((bf16[128,2048]{1,0:T(8,128)(2,1)}), bf16[4096,2048]{1,0:T(8,128)(2,1)}) %all-gather.3.cloned.1.call-update) | async-done | bytes 16777232 | tf_op jit(solution)/shard_map/all_gather | solution.py:18
  136.2 3.0 %fusion = f32[32,512]{1,0:T(8,128)S(1)} fusion(bf16[4096,2048]{1,0:T(8,128)(2,1)} %all-gather.3.cloned.1.call-done, f32[4096]{0:T(1024)S(1)} %convert_element_type.43, bf16[32,32,128]{2,1,0:T(8,128)(2,1)S(1)} %all-to-all-done), kind=kOutput, calls=%fused_computation | convolution fusion | flops 134610944 | bytes 4538368 | tf_op jit(solution)/shard_map/dot_general | solution.py:129
  139.2 3.0 %fusion.2 = f32[32,512]{1,0:T(8,128)S(1)} fusion(bf16[4096,2048]{1,0:T(8,128)(2,1)} %all-gather.3.cloned.1.call-done, f32[4096]{0:T(1024)S(1)} %convert_element_type.43, bf16[32,32,128]{2,1,0:T(8,128)(2,1)S(1)} %all-to-all-done), kind=kOutput, calls=%fused_computation.2 | convolution fusion | flops 134610944 | bytes 4538368 | tf_op jit(solution)/shard_map/dot_general | solution.py:129
  142.2 3.0 %fusion.4 = f32[32,512]{1,0:T(8,128)S(1)} fusion(bf16[4096,2048]{1,0:T(8,128)(2,1)} %all-gather.3.cloned.1.call-done, f32[4096]{0:T(1024)S(1)} %convert_element_type.43, bf16[32,32,128]{2,1,0:T(8,128)(2,1)S(1)} %all-to-all-done), kind=kOutput, calls=%fused_computation.4 | convolution fusion | flops 134610944 | bytes 4538368 | tf_op jit(solution)/shard_map/dot_general | solution.py:129
  145.2 3.0 %fusion.6 = f32[32,512]{1,0:T(8,128)S(1)} fusion(bf16[4096,2048]{1,0:T(8,128)(2,1)} %all-gather.3.cloned.1.call-done, f32[4096]{0:T(1024)S(1)} %convert_element_type.43, bf16[32,32,128]{2,1,0:T(8,128)(2,1)S(1)} %all-to-all-done), kind=kOutput, calls=%fused_computation.6 | convolution fusion | flops 134610944 | bytes 4538368 | tf_op jit(solution)/shard_map/dot_general | solution.py:129
  148.9 0.4 convolution_multiply_fusion.1
  149.3 0.4 fusion.9
  151.1 0.3 multiply_subtract_fusion
  151.6 1.9 convolution_subtract_fusion
  153.4 1.9 fusion.34
  155.3 0.4 fusion.80
  156.2 26.2 %all_gather.10 = bf16[16,32,512]{2,1,0:T(8,128)(2,1)} all-gather(bf16[1,32,512]{2,1,0:T(8,128)(2,1)S(1)} %convert_element_type.48), channel_id=1, replica_groups=mesh['grp'=2,'kv_0'=16,'kv_1'=2,'tp'=4] {'kv_0'}, dimensions={0}, use_global_device_ids=true | all-gather | bytes 557056 | tf_op jit(solution)/shard_map/all_gather | solution.py:30
  182.5 25.5 %all-gather.5.cloned.1.call-done = bf16[32,32,512]{2,1,0:T(8,128)(2,1)} async-done(((bf16[16,32,512]{2,1,0:T(8,128)(2,1)}), bf16[32,32,512]{2,1,0:T(8,128)(2,1)}) %all-gather.5.cloned.1.call-update) | async-done | bytes 1048592 | tf_op jit(solution)/shard_map/all_gather | solution.py:30
  208.0 1.3 copy.398
  209.3 0.4 fusion.81
  209.7 1.5 broadcast_in_dim.79
  211.2 4.5 %all-to-all-start.1 = ((f32[4,1024,128]{2,1,0:T(8,128)}), f32[4,1024,128]{2,1,0:T(8,128)}, u32[]{:S(2)}, u32[]{:S(2)}) async-start(f32[4,1024,128]{2,1,0:T(8,128)} %broadcast_in_dim.79), calls=%async_computation.1 | async-start | bytes 4194304 | tf_op jit(solution)/shard_map/all_to_all | solution.py:43
  215.7 1.9 reshape.149
  217.6 24.3 %all-to-all-done.1 = f32[4,1024,128]{2,1,0:T(8,128)} async-done(((f32[4,1024,128]{2,1,0:T(8,128)}), f32[4,1024,128]{2,1,0:T(8,128)}, u32[]{:S(2)}, u32[]{:S(2)}) %all-to-all-start.1) | async-done | bytes 2097184 | tf_op jit(solution)/shard_map/all_to_all | solution.py:43
  241.9 2.5 reduce_sum.59
  (99 shorter events, 5.3 us)
Async XLA Ops:
  7.2 202.1 %copy-start = (bf16[512,128]{1,0:T(8,128)(2,1)S(1)}, bf16[512,128]{1,0:T(8,128)(2,1)}, u32[]{:S(2)}) copy-start(bf16[512,128]{1,0:T(8,128)(2,1)} %param.27) | copy-start | bytes 393220
  7.2 27.8 %copy-start.9 = (s32[8]{0:T(128)S(1)}, s32[8]{0:T(128)}, u32[]{:S(2)}) copy-start(s32[8]{0:T(128)} %param.33) | copy-start | bytes 100
  7.2 27.8 %copy-start.5 = (f32[8,4,4]{0,2,1:T(4,128)S(1)}, f32[8,4,4]{0,2,1:T(4,128)}, u32[]{:S(2)}) copy-start(f32[8,4,4]{0,2,1:T(4,128)} %param.31) | copy-start | bytes 1540
  7.2 27.9 %copy-start.6 = (f32[8,4,4]{0,2,1:T(4,128)S(1)}, f32[8,4,4]{0,2,1:T(4,128)}, u32[]{:S(2)}) copy-start(f32[8,4,4]{0,2,1:T(4,128)} %param.32) | copy-start | bytes 1540
  7.2 28.2 %copy-start.2 = (bf16[8,4,512]{2,1,0:T(4,128)(2,1)S(1)}, bf16[8,4,512]{2,1,0:T(4,128)(2,1)}, u32[]{:S(2)}) copy-start(bf16[8,4,512]{2,1,0:T(4,128)(2,1)} %param.29) | copy-start | bytes 98308
  7.2 28.8 %copy-start.3 = (bf16[8,4,512]{2,1,0:T(4,128)(2,1)S(1)}, bf16[8,4,512]{2,1,0:T(4,128)(2,1)}, u32[]{:S(2)}) copy-start(bf16[8,4,512]{2,1,0:T(4,128)(2,1)} %param.30) | copy-start | bytes 98308
  7.2 29.2 %copy-start.4 = (bf16[4096]{0:T(1024)(128)(2,1)S(1)}, bf16[4096]{0:T(1024)(128)(2,1)}, u32[]{:S(2)}) copy-start(bf16[4096]{0:T(1024)(128)(2,1)} %param.18) | copy-start | bytes 24580
  7.3 29.2 %copy-start.10 = (bf16[128]{0:T(256)(128)(2,1)S(1)}, bf16[128]{0:T(256)(128)(2,1)}, u32[]{:S(2)}) copy-start(bf16[128]{0:T(256)(128)(2,1)} %param.26) | copy-start | bytes 772
  7.3 29.2 %copy-start.11 = (f32[4]{0:T(128)S(1)}, f32[4]{0:T(128)}, u32[]{:S(2)}) copy-start(f32[4]{0:T(128)} %param.25) | copy-start | bytes 52
  7.3 128.9 %all-gather.3.cloned.1.call-start = ((), (), s32[]{:S(2)}) async-start(), calls=%async_computation.2 | async-start | bytes 17301504 | tf_op jit(solution)/shard_map/all_gather | solution.py:18
  9.4 48.8 %all-to-all-start = ((bf16[32,32,128]{2,1,0:T(8,128)(2,1)}), bf16[32,32,128]{2,1,0:T(8,128)(2,1)S(1)}, u32[]{:S(2)}, u32[]{:S(2)}) async-start(bf16[32,32,128]{2,1,0:T(8,128)(2,1)} %bitcast.155), calls=%async_computation | async-start | bytes 524288 | tf_op jit(solution)/shard_map/all_to_all | solution.py:124
  34.9 173.1 %all-gather.5.cloned.1.call-start = ((), (), s32[]{:S(2)}) async-start(), calls=%async_computation.3 | async-start | bytes 1572864 | tf_op jit(solution)/shard_map/all_gather | solution.py:30
  39.2 1.8 copy-start.1
  42.8 15.6 %copy-start.7 = (bf16[4096,4]{0,1:T(4,128)(2,1)S(1)}, bf16[4096,4]{0,1:T(4,128)(2,1)}, u32[]{:S(2)}) copy-start(bf16[4096,4]{0,1:T(4,128)(2,1)} %param.24) | copy-start | bytes 98308
  42.8 15.6 %copy-start.8 = (bf16[4096,4]{0,1:T(4,128)(2,1)S(1)}, bf16[4096,4]{0,1:T(4,128)(2,1)}, u32[]{:S(2)}) copy-start(bf16[4096,4]{0,1:T(4,128)(2,1)} %param.23) | copy-start | bytes 98308
  211.2 30.7 %all-to-all-start.1 = ((f32[4,1024,128]{2,1,0:T(8,128)}), f32[4,1024,128]{2,1,0:T(8,128)}, u32[]{:S(2)}, u32[]{:S(2)}) async-start(f32[4,1024,128]{2,1,0:T(8,128)} %broadcast_in_dim.79), calls=%async_computation.1 | async-start | bytes 4194304 | tf_op jit(solution)/shard_map/all_to_all | solution.py:43
Sparse Core Ops, SparseCore 0:
  10.0 126.1 all-gather.2
  182.6 25.3 all-gather.4
where the time goes:
time: 252 us; the launch traced here: 251 us
  waiting for transfers between devices  137 us (54%)
  starting transfers between devices  30.2 us (12%)
  blocking collectives  26.2 us (10%)
  matrix products  25.2 us (10%)
  between operations  14.6 us (6%)
  local copies, waits for them, and re-layouts  11 us (4%)
  other arithmetic  7.45 us (3%)
    all_gather x1, waiting for transfers between devices, side_by_side(): lax.all_gather(both, axis, axis=dim, tiled=True)  76.6 us
    all_gather x1, blocking collectives, gather_in_order(): tiles = lax.all_gather(tiles, axes[k], axis=0, tiled=True)  26.2 us
    all_to_all x1, starting transfers between devices, per_device(): lax.all_to_all(hidden, KV, split_axis=0, concat_axis=1, tiled=True)  25.5 us
    all_gather x1, waiting for transfers between devices, gather_in_order(): tiles = lax.all_gather(tiles, axes[k], axis=0, tiled=True)  25.5 us
    all_to_all x1, waiting for transfers between devices, from_everyone(): return lax.all_to_all(copies, axis, split_axis=0, concat_axis=0, tiled=True)  24.3 us
    dot_general x4, matrix products, per_device(): jnp.dot(scaled, piece, preferred_element_type=jnp.float32)  12 us
    all_to_all x1, waiting for transfers between devices, per_device(): lax.all_to_all(hidden, KV, split_axis=0, concat_axis=1, tiled=True)  10.1 us
    dot_general x1, matrix products, delta_block(): jnp.einsum('shpk,shpv->shkv', keys * jnp.exp(final - totals)[..., None],...  5.32 us
  transfers between devices with their start and end apart: 4, of which 4 were waited for; matrix products, arithmetic and copies ran while one was open for 6% of the time, Pallas kernels for 0%

commit v1 on v0

--- a/solution.py
+++ b/solution.py
@@ -27,7 +27,11 @@
 def gather_in_order(value, axes, turns):
     tiles = value[None]
     for k in turns:
-        tiles = lax.all_gather(tiles, axes[k], axis=0, tiled=True)
+        matrix = axes[k]
+        mid_arr = lax.axis_size(matrix)
+        seen_now = jnp.stack(mid_arr * [tiles])
+        r2 = lax.all_to_all(seen_now, split_axis=0, axis_name=matrix, concat_axis=0)
+        tiles = jnp.concatenate(r2, axis=0)
     block = [lax.axis_size(axes[k]) for k in reversed(turns)]
     tiles = tiles.reshape(*block, *value.shape)
     turned = sorted(range(len(turns)), key=lambda place: turns[len(turns) - 1 - place])

time: 252 us -> 242 us (0.960)
  waiting for transfers between devices: 137 us -> 111 us
  blocking collectives: 26.2 us -> 42.7 us
    all_to_all x0 -> x2, blocking collectives: none -> 42.7 us  [gather_in_order(): r2 = lax.all_to_all(seen_now, split_axis=0, axis_name=matrix, concat_axis=0)]
    all_gather x1 -> x0, blocking collectives: 26.2 us -> none  [gather_in_order(): tiles = lax.all_gather(tiles, axes[k], axis=0, tiled=True)]
    all_gather x1 -> x0, waiting for transfers between devices: 25.5 us -> none  [gather_in_order(): tiles = lax.all_gather(tiles, axes[k], axis=0, tiled=True)]
  transfers between devices with their start and end apart: 4 -> 3, of which waited for: 4 -> 3; matrix products, arithmetic and copies ran while one was open for 6% -> 7% of each run, Pallas kernels for 0% -> 0%
where the time goes in v1:
time: 242 us; the launch traced here: 241 us
  waiting for transfers between devices  111 us (46%)
  blocking collectives  42.7 us (18%)
  starting transfers between devices  30.1 us (12%)
  matrix products  25.2 us (10%)
  between operations  14.6 us (6%)
  local copies, waits for them, and re-layouts  9.83 us (4%)
  other arithmetic  7.53 us (3%)
    all_gather x1, waiting for transfers between devices, side_by_side(): lax.all_gather(both, axis, axis=dim, tiled=True)  76.7 us
    all_to_all x2, blocking collectives, gather_in_order(): r2 = lax.all_to_all(seen_now, split_axis=0, axis_name=matrix, concat_axis=0)  42.7 us
    all_to_all x1, starting transfers between devices, per_device(): lax.all_to_all(hidden, KV, split_axis=0, concat_axis=1, tiled=True)  25.5 us
    all_to_all x1, waiting for transfers between devices, from_everyone(): return lax.all_to_all(copies, axis, split_axis=0, concat_axis=0, tiled=True)  24.2 us
    dot_general x4, matrix products, per_device(): jnp.dot(scaled, piece, preferred_element_type=jnp.float32)  12 us
    all_to_all x1, waiting for transfers between devices, per_device(): lax.all_to_all(hidden, KV, split_axis=0, concat_axis=1, tiled=True)  10.1 us
    dot_general x1, matrix products, delta_block(): jnp.einsum('shpk,shpv->shkv', keys * jnp.exp(final - totals)[..., None],...  5.32 us
  transfers between devices with their start and end apart: 3, of which 3 were waited for; matrix products, arithmetic and copies ran while one was open for 7% of the time, Pallas kernels for 0%

profile of v1, /device:TPU:33, one launch (start us, length us, event | category | flops | bytes accessed | tf_op | source)
XLA Modules:
  0.0 241.0 jit_solution(6642423522985516015)
XLA Ops:
  7.3 2.0 pad_maximum_fusion.1
  9.4 25.5 %all-to-all-start = ((bf16[32,32,128]{2,1,0:T(8,128)(2,1)}), bf16[32,32,128]{2,1,0:T(8,128)(2,1)S(1)}, u32[]{:S(2)}, u32[]{:S(2)}) async-start(bf16[32,32,128]{2,1,0:T(8,128)(2,1)} %bitcast.160), calls=%async_computation | async-start | bytes 524288 | tf_op jit(solution)/shard_map/all_to_all | solution.py:128
  35.5 0.4 fusion.11
  36.2 0.2 fusion.79
  36.4 2.7 %reshape.136 = f32[8,4,128,128]{3,2,1,0:T(8,128)S(1)} reshape(f32[8,4,16384]{2,1,0:T(4,128)} %param.28) | data formatting | bytes 4194304 | tf_op jit(solution)/shard_map/reshape | solution.py:170
  40.4 0.3 multiply_subtract_fusion.2
  40.8 1.9 convolution_subtract_fusion.1
  42.7 5.3 %multiply_add_fusion = f32[8,4,128,128]{3,2,1,0:T(8,128)S(1)} fusion(f32[8,4,128,128]{3,2,1,0:T(8,128)} %copy-done.1, f32[8,4,4,128]{3,2,1,0:T(4,128)S(1)} %convolution_subtract_fusion.1, f32[8,4]{1,0:T(8,128)S(1)} %copy.306, bf16[8,4,512]{2,1,0:T(4,128)(2,1)S(1)} %copy-done.2, f32[8,4,4]{2,1,0:T(4,128)S(1)} %copy.307, f32[8,4,4]{2,1,0:T(4,128)S(1)} %add_rsqrt_fusion.2), kind=kOutput, calls=%fused_computation.8 | convolution fusion | flops 26263552 | bytes 4293760 | tf_op jit(solution)/shard_map/shpk,shpv->shkv/dot_general | solution.py:97
  48.0 10.1 %all-to-all-done = bf16[32,32,128]{2,1,0:T(8,128)(2,1)S(1)} async-done(((bf16[32,32,128]{2,1,0:T(8,128)(2,1)}), bf16[32,32,128]{2,1,0:T(8,128)(2,1)S(1)}, u32[]{:S(2)}, u32[]{:S(2)}) %all-to-all-start) | async-done | bytes 262176 | tf_op jit(solution)/shard_map/all_to_all | solution.py:128
  58.2 0.2 fusion.12
  58.4 0.2 convolution_multiply_fusion.3
  58.7 0.7 reduce_window_sum.17
  59.5 76.7 %all-gather.2.cloned.1.call-done = bf16[4096,2048]{1,0:T(8,128)(2,1)} async-done(((bf16[128,2048]{1,0:T(8,128)(2,1)}), bf16[4096,2048]{1,0:T(8,128)(2,1)}) %all-gather.2.cloned.1.call-update) | async-done | bytes 16777232 | tf_op jit(solution)/shard_map/all_gather | solution.py:18
  136.2 3.0 %fusion = f32[32,512]{1,0:T(8,128)S(1)} fusion(bf16[4096,2048]{1,0:T(8,128)(2,1)} %all-gather.2.cloned.1.call-done, f32[4096]{0:T(1024)S(1)} %convert_element_type.41, bf16[32,32,128]{2,1,0:T(8,128)(2,1)S(1)} %all-to-all-done), kind=kOutput, calls=%fused_computation | convolution fusion | flops 134610944 | bytes 4538368 | tf_op jit(solution)/shard_map/dot_general | solution.py:133
  139.2 3.0 %fusion.2 = f32[32,512]{1,0:T(8,128)S(1)} fusion(bf16[4096,2048]{1,0:T(8,128)(2,1)} %all-gather.2.cloned.1.call-done, f32[4096]{0:T(1024)S(1)} %convert_element_type.41, bf16[32,32,128]{2,1,0:T(8,128)(2,1)S(1)} %all-to-all-done), kind=kOutput, calls=%fused_computation.2 | convolution fusion | flops 134610944 | bytes 4538368 | tf_op jit(solution)/shard_map/dot_general | solution.py:133
  142.2 3.0 %fusion.4 = f32[32,512]{1,0:T(8,128)S(1)} fusion(bf16[4096,2048]{1,0:T(8,128)(2,1)} %all-gather.2.cloned.1.call-done, f32[4096]{0:T(1024)S(1)} %convert_element_type.41, bf16[32,32,128]{2,1,0:T(8,128)(2,1)S(1)} %all-to-all-done), kind=kOutput, calls=%fused_computation.4 | convolution fusion | flops 134610944 | bytes 4538368 | tf_op jit(solution)/shard_map/dot_general | solution.py:133
  145.2 3.0 %fusion.6 = f32[32,512]{1,0:T(8,128)S(1)} fusion(bf16[4096,2048]{1,0:T(8,128)(2,1)} %all-gather.2.cloned.1.call-done, f32[4096]{0:T(1024)S(1)} %convert_element_type.41, bf16[32,32,128]{2,1,0:T(8,128)(2,1)S(1)} %all-to-all-done), kind=kOutput, calls=%fused_computation.6 | convolution fusion | flops 134610944 | bytes 4538368 | tf_op jit(solution)/shard_map/dot_general | solution.py:133
  148.9 0.4 convolution_multiply_fusion.1
  149.3 0.4 fusion.9
  149.8 0.2 fusion.78
  151.1 0.3 multiply_subtract_fusion
  151.6 1.9 convolution_subtract_fusion
  153.4 1.9 fusion.34
  155.3 0.4 fusion.80
  156.2 31.4 %all_to_all.28 = bf16[16,1,32,512]{3,2,1,0:T(8,128)(2,1)S(1)} all-to-all(bf16[16,1,32,512]{3,2,1,0:T(8,128)(2,1)S(1)} %stack.20), channel_id=1, replica_groups=mesh['grp'=2,'kv_0'=16,'kv_1'=2,'tp'=4] {'kv_0'}, dimensions={0} | all-to-all | bytes 1048576 | tf_op jit(solution)/shard_map/all_to_all | solution.py:33
  187.7 11.4 %all_to_all.29 = bf16[2,16,32,512]{3,2,1,0:T(8,128)(2,1)S(1)} all-to-all(bf16[2,16,32,512]{3,2,1,0:T(8,128)(2,1)S(1)} %pad_maximum_fusion), channel_id=1, replica_groups=mesh['grp'=2,'kv_0'=16,'kv_1'=2,'tp'=4] {'kv_1'}, dimensions={0} | all-to-all | bytes 2097152 | tf_op jit(solution)/shard_map/all_to_all | solution.py:33
  199.2 0.4 fusion.81
  199.6 1.4 broadcast_in_dim.78
  201.0 4.5 %all-to-all-start.3 = ((f32[4,1024,128]{2,1,0:T(8,128)}), f32[4,1024,128]{2,1,0:T(8,128)}, u32[]{:S(2)}, u32[]{:S(2)}) async-start(f32[4,1024,128]{2,1,0:T(8,128)} %broadcast_in_dim.78), calls=%async_computation.3 | async-start | bytes 4194304 | tf_op jit(solution)/shard_map/all_to_all | solution.py:47
  205.6 1.9 reshape.143
  207.4 24.2 %all-to-all-done.3 = f32[4,1024,128]{2,1,0:T(8,128)} async-done(((f32[4,1024,128]{2,1,0:T(8,128)}), f32[4,1024,128]{2,1,0:T(8,128)}, u32[]{:S(2)}, u32[]{:S(2)}) %all-to-all-start.3) | async-done | bytes 2097184 | tf_op jit(solution)/shard_map/all_to_all | solution.py:47
  231.6 2.5 %reduce_sum.59 = bf16[1024,128]{1,0:T(8,128)(2,1)} reduce(f32[4,1024,128]{2,1,0:T(8,128)} %all-to-all-done.3, f32[]{:T(128)} %constant.18.clone.1), dimensions={0}, to_apply=%region_7.8 | reduce | flops 393216 | bytes 2359300 | tf_op jit(solution)/shard_map/reduce_sum | solution.py:51
  (99 shorter events, 5.3 us)
Async XLA Ops:
  7.2 192.0 %copy-start = (bf16[512,128]{1,0:T(8,128)(2,1)S(1)}, bf16[512,128]{1,0:T(8,128)(2,1)}, u32[]{:S(2)}) copy-start(bf16[512,128]{1,0:T(8,128)(2,1)} %param.27) | copy-start | bytes 393220
  7.2 27.7 %copy-start.9 = (s32[8]{0:T(128)S(1)}, s32[8]{0:T(128)}, u32[]{:S(2)}) copy-start(s32[8]{0:T(128)} %param.33) | copy-start | bytes 100
  7.2 27.7 %copy-start.5 = (f32[8,4,4]{0,2,1:T(4,128)S(1)}, f32[8,4,4]{0,2,1:T(4,128)}, u32[]{:S(2)}) copy-start(f32[8,4,4]{0,2,1:T(4,128)} %param.31) | copy-start | bytes 1540
  7.2 27.8 %copy-start.6 = (f32[8,4,4]{0,2,1:T(4,128)S(1)}, f32[8,4,4]{0,2,1:T(4,128)}, u32[]{:S(2)}) copy-start(f32[8,4,4]{0,2,1:T(4,128)} %param.32) | copy-start | bytes 1540
  7.2 28.1 %copy-start.2 = (bf16[8,4,512]{2,1,0:T(4,128)(2,1)S(1)}, bf16[8,4,512]{2,1,0:T(4,128)(2,1)}, u32[]{:S(2)}) copy-start(bf16[8,4,512]{2,1,0:T(4,128)(2,1)} %param.29) | copy-start | bytes 98308
  7.2 28.7 %copy-start.3 = (bf16[8,4,512]{2,1,0:T(4,128)(2,1)S(1)}, bf16[8,4,512]{2,1,0:T(4,128)(2,1)}, u32[]{:S(2)}) copy-start(bf16[8,4,512]{2,1,0:T(4,128)(2,1)} %param.30) | copy-start | bytes 98308
  7.2 29.1 %copy-start.4 = (bf16[4096]{0:T(1024)(128)(2,1)S(1)}, bf16[4096]{0:T(1024)(128)(2,1)}, u32[]{:S(2)}) copy-start(bf16[4096]{0:T(1024)(128)(2,1)} %param.18) | copy-start | bytes 24580
  7.3 29.1 %copy-start.10 = (bf16[128]{0:T(256)(128)(2,1)S(1)}, bf16[128]{0:T(256)(128)(2,1)}, u32[]{:S(2)}) copy-start(bf16[128]{0:T(256)(128)(2,1)} %param.26) | copy-start | bytes 772
  7.3 29.1 %copy-start.11 = (f32[4]{0:T(128)S(1)}, f32[4]{0:T(128)}, u32[]{:S(2)}) copy-start(f32[4]{0:T(128)} %param.25) | copy-start | bytes 52
  7.3 128.9 %all-gather.2.cloned.1.call-start = ((), (), s32[]{:S(2)}) async-start(), calls=%async_computation.4 | async-start | bytes 17301504 | tf_op jit(solution)/shard_map/all_gather | solution.py:18
  9.4 48.8 %all-to-all-start = ((bf16[32,32,128]{2,1,0:T(8,128)(2,1)}), bf16[32,32,128]{2,1,0:T(8,128)(2,1)S(1)}, u32[]{:S(2)}, u32[]{:S(2)}) async-start(bf16[32,32,128]{2,1,0:T(8,128)(2,1)} %bitcast.160), calls=%async_computation | async-start | bytes 524288 | tf_op jit(solution)/shard_map/all_to_all | solution.py:128
  39.1 1.8 copy-start.1
  42.7 15.7 %copy-start.7 = (bf16[4096,4]{0,1:T(4,128)(2,1)S(1)}, bf16[4096,4]{0,1:T(4,128)(2,1)}, u32[]{:S(2)}) copy-start(bf16[4096,4]{0,1:T(4,128)(2,1)} %param.24) | copy-start | bytes 98308
  42.7 15.7 %copy-start.8 = (bf16[4096,4]{0,1:T(4,128)(2,1)S(1)}, bf16[4096,4]{0,1:T(4,128)(2,1)}, u32[]{:S(2)}) copy-start(bf16[4096,4]{0,1:T(4,128)(2,1)} %param.23) | copy-start | bytes 98308
  201.0 30.6 %all-to-all-start.3 = ((f32[4,1024,128]{2,1,0:T(8,128)}), f32[4,1024,128]{2,1,0:T(8,128)}, u32[]{:S(2)}, u32[]{:S(2)}) async-start(f32[4,1024,128]{2,1,0:T(8,128)} %broadcast_in_dim.78), calls=%async_computation.3 | async-start | bytes 4194304 | tf_op jit(solution)/shard_map/all_to_all | solution.py:47
Sparse Core Ops, SparseCore 0:
  10.0 126.1 all-gather.1
